TPU v7x, 32 devices: a whole 2x2x4 slice. The times are simulated.
32 devices in a mesh: sp: 16 (over z, y, x), tp: 2 (over core).
Axes of the slice: x: 2, y: 2, z: 4, core: 2. Of those that a mesh axis runs over, the one named last changes fastest.
Arguments:
- value_in: bfloat16 [4096, 2048], P('sp', 'tp'), may hold values from -25 to 25, as said below
- gate_in: bfloat16 [4096, 2048], P('sp', 'tp'), may hold values from -6 to 6
- taps: float32 [31, 2048], P(None, 'tp'), may hold values from -1 to 1
- gain: float32 [2048], P('tp'), may hold values from 0.1 to 1.9
- shift: float32 [2048], P('tp'), may hold values from -3 to 3
- w_out: bfloat16 [2048, 2048], P('tp'), may hold values from -0.125 to 0.125
- grad_out: bfloat16 [4096, 2048], P('sp'), may hold values from -6 to 6
Outputs:
- d_value: bfloat16 [4096, 2048], P('sp', 'tp')
- d_gate: bfloat16 [4096, 2048], P('sp', 'tp')
- d_taps: float32 [31, 2048], P(None, 'tp')
- d_gain: float32 [2048], P('tp')
- d_shift: float32 [2048], P('tp')
Inputs may be any that keep to these rules, and one draw needn't show every extreme that they name: `value_in`: channel blocks of different magnitude.
All inputs are finite; a program needn't handle non-finite values.
Results may differ from a plain program's by a relative error of at most 0.007.
Values may be sent and summed in bfloat16 or wider, within the bound.
No kernel may reach another device: no remote copies, remote signals or barrier semaphores. Data moves between devices by JAX's collectives and lax.ppermute only.
A program may use at most 64 MiB of HBM per device.

v0:
```python
import math

import jax
import jax.numpy as jnp
from jax import lax
from jax.sharding import PartitionSpec as P

EPS = 1e-05


def with_halo(block, sides, width):
    for axis, dim in sides:
        count = lax.axis_size(axis)
        forward = [(i, i + 1) for i in range(count - 1)]
        backward = [(target, source) for source, target in forward]
        low = lax.ppermute(
            lax.slice_in_dim(block, block.shape[dim] - width, None, axis=dim), axis, forward
        )
        high = lax.ppermute(lax.slice_in_dim(block, 0, width, axis=dim), axis, backward)
        block = jnp.concatenate([low, block, high], axis=dim)
    return block


def gated_rows(value_rows, gate_rows):
    gate_sig = jax.nn.sigmoid(gate_rows.astype(jnp.float32))
    return ((value_rows.astype(jnp.float32) * gate_sig).astype(jnp.bfloat16), gate_sig)


def convolve(window, taps, count):
    wide = window.astype(jnp.float32)
    total = jnp.zeros((count, wide.shape[1]), jnp.float32)
    for offset in range(taps.shape[0]):
        total = total + taps[offset] * wide[offset : offset + count]
    return total


def norm_backward(conv_out, grad_rows, gain, shift, w_out, width):
    sums, squares = lax.psum((jnp.sum(conv_out, 1), jnp.sum(conv_out * conv_out, 1)), "tp")
    mean = sums / width
    var = squares / width - mean * mean
    inv = lax.rsqrt(var + EPS)
    normed = (conv_out - mean[:, None]) * inv[:, None]
    pre = normed * gain + shift
    grad_mix = lax.dot_general(
        grad_rows, w_out, (((1,), (1,)), ((), ())), preferred_element_type=jnp.float32
    )
    sig = jax.nn.sigmoid(pre)
    grad_pre = grad_mix * sig * (1.0 + pre * (1.0 - sig))
    grad_normed = grad_pre * gain
    first, second = lax.psum((jnp.sum(grad_normed, 1), jnp.sum(grad_normed * normed, 1)), "tp")
    grad_conv = inv[:, None] * (
        grad_normed - first[:, None] / width - normed * second[:, None] / width
    )
    return (grad_conv, grad_pre, normed)


def shards(value_in, gate_in, taps, gain, shift, w_out, grad_out):
    half = taps.shape[0] // 2
    kernel = taps.shape[0]
    rows = value_in.shape[0]
    width = value_in.shape[1] * lax.axis_size("tp")
    total = rows * lax.axis_size("sp")
    gated, gate_sig = gated_rows(value_in, gate_in)
    gated_wide = with_halo(gated, (("sp", 0),), half)
    conv_out = convolve(gated_wide, taps, rows)
    grad_conv, grad_pre, normed = norm_backward(conv_out, grad_out, gain, shift, w_out, width)
    grad_wide = with_halo(grad_conv, (("sp", 0),), half)
    own_grad = grad_wide[half : half + rows]
    gated_float = gated_wide.astype(jnp.float32)
    grad_gated = jnp.zeros((rows, own_grad.shape[1]), jnp.float32)
    for offset in range(kernel):
        grad_gated = (
            grad_gated + taps[offset] * grad_wide[2 * half - offset : 2 * half - offset + rows]
        )
    tap_terms = jnp.stack(
        [jnp.sum(own_grad * gated_float[offset : offset + rows], 0) for offset in range(kernel)]
    )
    scale = 1.0 / math.sqrt(total)
    stacked = (
        jnp.concatenate(
            [tap_terms, jnp.sum(grad_pre * normed, 0)[None], jnp.sum(grad_pre, 0)[None]], 0
        )
        * scale
    )
    summed = lax.psum(stacked, "sp")
    d_taps = summed[:kernel]
    d_gain = summed[kernel]
    d_shift = summed[kernel + 1]
    d_value = (grad_gated * gate_sig).astype(jnp.bfloat16)
    d_gate = (grad_gated * value_in.astype(jnp.float32) * gate_sig * (1.0 - gate_sig)).astype(
        jnp.bfloat16
    )
    return (d_value, d_gate, d_taps, d_gain, d_shift)


def solution(mesh):
    return jax.shard_map(
        shards,
        mesh=mesh,
        in_specs=(
            P("sp", "tp"),
            P("sp", "tp"),
            P(None, "tp"),
            P("tp"),
            P("tp"),
            P("tp", None),
            P("sp", None),
        ),
        out_specs=(P("sp", "tp"), P("sp", "tp"), P(None, "tp"), P("tp"), P("tp")),
        check_vma=False,
    )
```

profile of v0, /device:TPU:0, one launch (start us, length us, event | category | flops | bytes accessed | tf_op | source)
XLA Modules:
  0.0 175.2 jit_solution(298959568165321427)
XLA Ops:
  7.2 0.0 copy-start
  7.2 0.0 all-reduce.4.cloned.1.call-start
  7.2 1.6 fusion.1
  8.9 4.9 %collective-permute-start = (bf16[15,1024]{1,0:T(8,128)(2,1)S(1)}, bf16[15,1024]{1,0:T(8,128)(2,1)S(1)}, u32[]{:S(2)}, u32[]{:S(2)}) collective-permute-start(bf16[15,1024]{1,0:T(8,128)(2,1)S(1)} %get-tuple-element.52), channel_id=1, source_target_pairs={{0,2},{2,4},{4,6},{6,8},{8,10},{10,12},{12,14},{14,16},{16,18},{18... | collective-permute-start | bytes 92168 | tf_op jit(solution)/shard_map/ppermute | solution.py:16
  13.7 1.3 collective-permute-start.1
  15.0 0.1 fusion.97
  15.2 0.0 copy-start.12
  15.2 0.0 copy-start.13
  15.3 0.0 collective-permute-done
  15.4 4.2 %collective-permute-done.1 = bf16[15,1024]{1,0:T(8,128)(2,1)S(1)} collective-permute-done((bf16[15,1024]{1,0:T(8,128)(2,1)S(1)}, bf16[15,1024]{1,0:T(8,128)(2,1)S(1)}, u32[]{:S(2)}, u32[]{:S(2)}) %collective-permute-start.1) | collective-permute-done | bytes 30752 | tf_op jit(solution)/shard_map/ppermute | solution.py:19
  19.5 0.2 maximum_convert_fusion
  19.7 0.0 copy-start.24
  19.7 0.0 copy-start.25
  19.7 5.7 %multiply_reduce_fusion.33 = (f32[256]{0:T(256)S(1)}, f32[256]{0:T(256)S(1)}, f32[256,1024]{1,0:T(8,128)S(1)}) fusion(f32[286,1024]{1,0:T(8,128)S(1)} %maximum_convert_fusion, f32[1024]{0:T(1024)S(1)} %bitcast.126, f32[1024]{0:T(1024)S(1)} %bitcast.128, f32[1024]{0:T(1024)S(1)} %bitcast.70, f32[1024]{0:T(1024)S(1)} %bitcast.72, f32[1024]{0:T(1024)S(1)} %bitcast.74, ...), kind=kLoop, calls=%fused_computation.186 | loop fusion | flops 16776704 | bytes 33683456 | tf_op jit(solution)/shard_map/reduce_sum | solution.py:38
  25.6 2.5 %all-reduce.1 = (f32[256]{0:T(256)S(1)}, f32[256]{0:T(256)S(1)}) all-reduce(f32[256]{0:T(256)S(1)} %get-tuple-element.41, f32[256]{0:T(256)S(1)} %get-tuple-element.40), channel_id=1, replica_groups=mesh['sp'=16,'tp'=2] {'tp'}, use_global_device_ids=true, to_apply=%region_3.0 | all-reduce | flops 512 | bytes 4096 | tf_op jit(solution)/shard_map/psum | solution.py:38
  28.1 5.5 %multiply_reduce_fusion = (f32[1024]{0:T(1024)}, f32[256]{0:T(256)S(1)}, f32[256]{0:T(256)S(1)}, f32[1024]{0:T(1024)}, f32[256,1024]{1,0:T(8,128)}) fusion(f32[256,1024]{1,0:T(8,128)S(1)} %get-tuple-element.49, f32[256]{0:T(256)S(1)} %get-tuple-element.88, f32[256]{0:T(256)S(1)} %get-tuple-element.87, f32[1024]{0:T(1024)S(1)} %copy-done.24, ...), kind=kOutput, calls=%fused_computation.150 | convolution fusion | flops 1078720000 | bytes 7360512 | tf_op jit(solution)/shard_map/dot_general | solution.py:44
  33.7 2.4 %all-reduce = (f32[256]{0:T(256)S(1)}, f32[256]{0:T(256)S(1)}) all-reduce(f32[256]{0:T(256)S(1)} %get-tuple-element.37, f32[256]{0:T(256)S(1)} %get-tuple-element.38), channel_id=1, replica_groups=mesh['sp'=16,'tp'=2] {'tp'}, use_global_device_ids=true, to_apply=%region_7.0 | all-reduce | flops 512 | bytes 4096 | tf_op jit(solution)/shard_map/psum | solution.py:50
  36.1 4.8 %multiply_reduce_fusion.1 = (f32[1024]{0:T(1024)}, f32[1024]{0:T(1024)}, f32[1024]{0:T(1024)}, f32[1024]{0:T(1024)}, f32[1024]{0:T(1024)}, /*index=5*/f32[1024]{...) fusion(f32[286,1024]{1,0:T(8,128)S(1)} %maximum_convert_fusion,, ...), kind=kLoop, calls=%fused_computation.151 | loop fusion | flops 11515904 | bytes 22102016 | tf_op jit(solution)/shard_map/reduce_sum | solution.py:76
  41.0 2.4 %multiply_reduce_fusion.2 = (f32[1024]{0:T(1024)}, f32[1024]{0:T(1024)}, f32[1024]{0:T(1024)}, f32[1024]{0:T(1024)}, f32[1024]{0:T(1024)}, /*index=5*/f32[1024]{...) fusion(f32[256,1024]{1,0:T(8,128)S(1)} %get-tuple-element.46, ...), kind=kLoop, calls=%fused_computation.152 | loop fusion | flops 6802432 | bytes 14733312 | tf_op jit(solution)/shard_map/reduce_sum | solution.py:76
  43.3 0.6 fusion.94
  44.0 1.3 collective-permute-start.2
  45.3 4.9 %collective-permute-start.3 = (f32[15,1024]{1,0:T(8,128)S(1)}, f32[15,1024]{1,0:T(8,128)S(1)}, u32[]{:S(2)}, u32[]{:S(2)}) collective-permute-start(f32[15,1024]{1,0:T(8,128)S(1)} %get-tuple-element.51), channel_id=1, source_target_pairs={{0,2},{2,4},{4,6},{6,8},{8,10},{10,12},{12,14},{14,16},{16,18},{18... | collective-permute-start | bytes 184328 | tf_op jit(solution)/shard_map/ppermute | solution.py:16
  50.2 3.8 %concatenate.44 = f32[33,1024]{1,0:T(8,128)S(1)} concatenate(f32[1,1024]{1,0:T(1,128)} %bitcast.160, f32[1,1024]{1,0:T(1,128)} %bitcast.159, f32[1,1024]{1,0:T(1,128)} %bitcast.158, f32[1,1024]{1,0:T(1,128)} %bitcast.157, f32[1,1024]{1,0:T(1,128)} %bitcast.156, f32[1,1024]{1,0:T(1,128)} %bitcast.155, f32[1,1024]{1,0:T(1,128)} %bitcast.154, f32[1,1024]{1,0:T(1,128)} %bitcast.153, ...), dimensions={0} | concatenate | bytes 270336 | tf_op jit(solution)/shard_map/concatenate | solution.py:80
  54.0 0.7 broadcast_multiply_fusion
  54.7 0.0 all-reduce.4.cloned.1.call-update
  54.7 0.0 collective-permute-done.2
  54.7 0.0 collective-permute-done.3
  54.8 6.9 %fusion.4 = (bf16[256,1024]{1,0:T(8,128)(2,1)}, f32[256,1024]{1,0:T(8,128)}) fusion(bf16[256,1024]{1,0:T(8,128)(2,1)S(1)} %copy-done.3, bf16[256,1024]{1,0:T(8,128)(2,1)S(1)} %copy-done.1, f32[256,1024]{1,0:T(8,128)S(1)} %get-tuple-element.46, f32[15,1024]{1,0:T(8,128)S(1)} %collective-permute-done.3, f32[1024]{0:T(1024)} %bitcast.127, f32[1024]{0:T(1024)} %bitcast.129, ...), kind=kLoop, calls=%fused_computation.35 | loop fusion | flops 26476544 | bytes 3919872 | tf_op jit(solution)/shard_map/convert_element_type | solution.py:90
  61.7 2.3 %multiply_convert_fusion = bf16[256,1024]{1,0:T(8,128)(2,1)} fusion(f32[256,1024]{1,0:T(8,128)} %get-tuple-element.48, bf16[256,1024]{1,0:T(8,128)(2,1)S(1)} %copy-done.1), kind=kLoop, calls=%fused_computation.182 | loop fusion | flops 1572864 | bytes 2097152 | tf_op jit(solution)/shard_map/convert_element_type | solution.py:89
  64.0 101.4 %all-reduce.4.cloned.1.call-done = f32[33,1024]{1,0:T(8,128)} async-done(((f32[33,1024]{1,0:T(8,128)}), f32[33,1024]{1,0:T(8,128)}) %all-reduce.4.cloned.1.call-update) | async-done | bytes 135184 | tf_op jit(solution)/shard_map/psum | solution.py:85
  165.4 1.4 fusion.96
  166.8 1.6 slice.579
  (51 shorter events, 0.2 us)
Async XLA Ops:
  7.2 20.9 %copy-start = (bf16[256,2048]{1,0:T(8,128)(2,1)S(1)}, bf16[256,2048]{1,0:T(8,128)(2,1)}, u32[]{:S(2)}) copy-start(bf16[256,2048]{1,0:T(8,128)(2,1)} %param.13) | copy-start | bytes 3145732
  7.2 7.9 %copy-start.4 = (f32[31,1024]{1,0:T(8,128)S(1)}, f32[31,1024]{1,0:T(8,128)}, u32[]{:S(2)}) copy-start(f32[31,1024]{1,0:T(8,128)} %param.9) | copy-start | bytes 380932
  7.2 158.2 %all-reduce.4.cloned.1.call-start = ((), (), s32[]{:S(2)}) async-start(), calls=%async_computation | async-start | bytes 327680 | tf_op jit(solution)/shard_map/psum | solution.py:85
  8.9 6.5 %collective-permute-start = (bf16[15,1024]{1,0:T(8,128)(2,1)S(1)}, bf16[15,1024]{1,0:T(8,128)(2,1)S(1)}, u32[]{:S(2)}, u32[]{:S(2)}) collective-permute-start(bf16[15,1024]{1,0:T(8,128)(2,1)S(1)} %get-tuple-element.52), channel_id=1, source_target_pairs={{0,2},{2,4},{4,6},{6,8},{8,10},{10,12},{12,14},{14,16},{16,18},{18... | collective-permute-start | bytes 92168 | tf_op jit(solution)/shard_map/ppermute | solution.py:16
  13.7 5.8 %collective-permute-start.1 = (bf16[15,1024]{1,0:T(8,128)(2,1)S(1)}, bf16[15,1024]{1,0:T(8,128)(2,1)S(1)}, u32[]{:S(2)}, u32[]{:S(2)}) collective-permute-start(bf16[15,1024]{1,0:T(8,128)(2,1)S(1)} %get-tuple-element.53), channel_id=1, source_target_pairs={{2,0},{4,2},{6,4},{8,6},{10,8},{12,10},{14,12},{16,14},{18,16},{20... | collective-permute-start | bytes 92168 | tf_op jit(solution)/shard_map/ppermute | solution.py:19
  15.1 10.3 %copy-start.5 = (f32[1,1024]{1,0:T(1,128)}, f32[1,1024]{1,0:T(1,128)S(1)}, u32[]{:S(2)}) copy-start(f32[1,1024]{1,0:T(1,128)S(1)} %get-tuple-element.68) | copy-start | bytes 12292
  15.1 10.3 %copy-start.6 = (f32[1,1024]{1,0:T(1,128)}, f32[1,1024]{1,0:T(1,128)S(1)}, u32[]{:S(2)}) copy-start(f32[1,1024]{1,0:T(1,128)S(1)} %get-tuple-element.69) | copy-start | bytes 12292
  15.1 10.3 %copy-start.7 = (f32[1,1024]{1,0:T(1,128)}, f32[1,1024]{1,0:T(1,128)S(1)}, u32[]{:S(2)}) copy-start(f32[1,1024]{1,0:T(1,128)S(1)} %get-tuple-element.70) | copy-start | bytes 12292
  15.1 10.3 %copy-start.8 = (f32[1,1024]{1,0:T(1,128)}, f32[1,1024]{1,0:T(1,128)S(1)}, u32[]{:S(2)}) copy-start(f32[1,1024]{1,0:T(1,128)S(1)} %get-tuple-element.71) | copy-start | bytes 12292
  15.1 10.3 %copy-start.9 = (f32[1,1024]{1,0:T(1,128)}, f32[1,1024]{1,0:T(1,128)S(1)}, u32[]{:S(2)}) copy-start(f32[1,1024]{1,0:T(1,128)S(1)} %get-tuple-element.72) | copy-start | bytes 12292
  15.2 10.3 %copy-start.10 = (f32[1,1024]{1,0:T(1,128)}, f32[1,1024]{1,0:T(1,128)S(1)}, u32[]{:S(2)}) copy-start(f32[1,1024]{1,0:T(1,128)S(1)} %get-tuple-element.73) | copy-start | bytes 12292
  15.2 10.3 %copy-start.11 = (f32[1,1024]{1,0:T(1,128)}, f32[1,1024]{1,0:T(1,128)S(1)}, u32[]{:S(2)}) copy-start(f32[1,1024]{1,0:T(1,128)S(1)} %get-tuple-element.74) | copy-start | bytes 12292
  15.2 10.3 %copy-start.12 = (f32[1,1024]{1,0:T(1,128)}, f32[1,1024]{1,0:T(1,128)S(1)}, u32[]{:S(2)}) copy-start(f32[1,1024]{1,0:T(1,128)S(1)} %get-tuple-element.75) | copy-start | bytes 12292
  15.2 10.3 %copy-start.13 = (f32[1,1024]{1,0:T(1,128)}, f32[1,1024]{1,0:T(1,128)S(1)}, u32[]{:S(2)}) copy-start(f32[1,1024]{1,0:T(1,128)S(1)} %get-tuple-element.76) | copy-start | bytes 12292
  15.2 10.3 %copy-start.14 = (f32[1,1024]{1,0:T(1,128)}, f32[1,1024]{1,0:T(1,128)S(1)}, u32[]{:S(2)}) copy-start(f32[1,1024]{1,0:T(1,128)S(1)} %get-tuple-element.77) | copy-start | bytes 12292
  15.3 10.3 %copy-start.15 = (f32[1,1024]{1,0:T(1,128)}, f32[1,1024]{1,0:T(1,128)S(1)}, u32[]{:S(2)}) copy-start(f32[1,1024]{1,0:T(1,128)S(1)} %get-tuple-element.78) | copy-start | bytes 12292
  15.3 10.3 %copy-start.16 = (f32[1,1024]{1,0:T(1,128)}, f32[1,1024]{1,0:T(1,128)S(1)}, u32[]{:S(2)}) copy-start(f32[1,1024]{1,0:T(1,128)S(1)} %get-tuple-element.79) | copy-start | bytes 12292
  15.3 10.3 %copy-start.17 = (f32[1,1024]{1,0:T(1,128)}, f32[1,1024]{1,0:T(1,128)S(1)}, u32[]{:S(2)}) copy-start(f32[1,1024]{1,0:T(1,128)S(1)} %get-tuple-element.80) | copy-start | bytes 12292
  15.3 10.3 %copy-start.18 = (f32[1,1024]{1,0:T(1,128)}, f32[1,1024]{1,0:T(1,128)S(1)}, u32[]{:S(2)}) copy-start(f32[1,1024]{1,0:T(1,128)S(1)} %get-tuple-element.81) | copy-start | bytes 12292
  15.3 10.3 %copy-start.19 = (f32[1,1024]{1,0:T(1,128)}, f32[1,1024]{1,0:T(1,128)S(1)}, u32[]{:S(2)}) copy-start(f32[1,1024]{1,0:T(1,128)S(1)} %get-tuple-element.82) | copy-start | bytes 12292
  15.3 10.3 %copy-start.20 = (f32[1,1024]{1,0:T(1,128)}, f32[1,1024]{1,0:T(1,128)S(1)}, u32[]{:S(2)}) copy-start(f32[1,1024]{1,0:T(1,128)S(1)} %get-tuple-element.83) | copy-start | bytes 12292
  15.3 10.3 %copy-start.21 = (f32[1,1024]{1,0:T(1,128)}, f32[1,1024]{1,0:T(1,128)S(1)}, u32[]{:S(2)}) copy-start(f32[1,1024]{1,0:T(1,128)S(1)} %get-tuple-element.84) | copy-start | bytes 12292
  15.3 10.3 %copy-start.22 = (f32[1,1024]{1,0:T(1,128)}, f32[1,1024]{1,0:T(1,128)S(1)}, u32[]{:S(2)}) copy-start(f32[1,1024]{1,0:T(1,128)S(1)} %get-tuple-element.85) | copy-start | bytes 12292
  15.3 10.3 %copy-start.23 = (f32[1,1024]{1,0:T(1,128)}, f32[1,1024]{1,0:T(1,128)S(1)}, u32[]{:S(2)}) copy-start(f32[1,1024]{1,0:T(1,128)S(1)} %get-tuple-element.86) | copy-start | bytes 12292
  19.7 8.4 %copy-start.24 = (f32[1024]{0:T(1024)S(1)}, f32[1024]{0:T(1024)}, u32[]{:S(2)}) copy-start(f32[1024]{0:T(1024)} %param.10) | copy-start | bytes 12292
  19.7 8.4 %copy-start.25 = (f32[1024]{0:T(1024)S(1)}, f32[1024]{0:T(1024)}, u32[]{:S(2)}) copy-start(f32[1024]{0:T(1024)} %param.11) | copy-start | bytes 12292
  25.6 8.0 %copy-start.2 = (f32[256,1024]{1,0:T(8,128)}, f32[256,1024]{1,0:T(8,128)S(1)}, u32[]{:S(2)}) copy-start(f32[256,1024]{1,0:T(8,128)S(1)} %get-tuple-element.49) | copy-start | bytes 3145732
  43.3 11.4 %copy-start.1 = (bf16[256,1024]{1,0:T(8,128)(2,1)S(1)}, bf16[256,1024]{1,0:T(8,128)(2,1)}, u32[]{:S(2)}) copy-start(bf16[256,1024]{1,0:T(8,128)(2,1)} %param.8) | copy-start | bytes 1572868
  43.3 11.4 %copy-start.3 = (bf16[256,1024]{1,0:T(8,128)(2,1)S(1)}, bf16[256,1024]{1,0:T(8,128)(2,1)}, u32[]{:S(2)}) copy-start(bf16[256,1024]{1,0:T(8,128)(2,1)} %param.7) | copy-start | bytes 1572868
  44.0 10.7 %collective-permute-start.2 = (f32[15,1024]{1,0:T(8,128)}, f32[15,1024]{1,0:T(8,128)S(1)}, u32[]{:S(2)}, u32[]{:S(2)}) collective-permute-start(f32[15,1024]{1,0:T(8,128)} %get-tuple-element.50), channel_id=1, source_target_pairs={{2,0},{4,2},{6,4},{8,6},{10,8},{12,10},{14,12},{16,14},{18,16},{20... | collective-permute-start | bytes 184328 | tf_op jit(solution)/shard_map/ppermute | solution.py:19
  45.3 9.5 %collective-permute-start.3 = (f32[15,1024]{1,0:T(8,128)S(1)}, f32[15,1024]{1,0:T(8,128)S(1)}, u32[]{:S(2)}, u32[]{:S(2)}) collective-permute-start(f32[15,1024]{1,0:T(8,128)S(1)} %get-tuple-element.51), channel_id=1, source_target_pairs={{0,2},{2,4},{4,6},{6,8},{8,10},{10,12},{12,14},{14,16},{16,18},{18... | collective-permute-start | bytes 184328 | tf_op jit(solution)/shard_map/ppermute | solution.py:16
Sparse Core Ops, SparseCore 0:
  54.8 110.4 all-reduce.3
where the time goes:
time: 176 us; the launch traced here: 175 us
  waiting for transfers between devices  106 us (60%)
  other arithmetic  24.5 us (14%)
  between operations  14.5 us (8%)
  starting transfers between devices  12.4 us (7%)
  local copies, waits for them, and re-layouts  7.63 us (4%)
  matrix products  5.53 us (3%)
  blocking collectives  4.91 us (3%)
    psum x1, waiting for transfers between devices, shards(): summed = lax.psum(stacked, 'sp')  101 us
    ppermute x2, starting transfers between devices, with_halo(): lax.ppermute(lax.slice_in_dim(block, block.shape[dim] - width, None, axis...  9.8 us
    reduce_sum x2, other arithmetic, shards(): jnp.sum(own_grad * gated_float[offset:offset + rows], 0)  7.23 us
    convert_element_type x1, other arithmetic, shards(): (grad_gated * value_in.astype(jnp.float32) * gate_sig * (1.0 - gate_sig))...  6.89 us
    reduce_sum x1, other arithmetic, norm_backward(): jnp.sum(conv_out * conv_out, 1)  5.69 us
    dot_general x1, matrix products, norm_backward(): lax.dot_general(grad_rows, w_out, (((1,), (1,)), ((), ())), preferred_ele...  5.53 us
    ppermute x2, waiting for transfers between devices, with_halo(): lax.ppermute(lax.slice_in_dim(block, 0, width, axis=dim), axis, backward)  4.19 us
    concatenate x1, local copies, waits for them, and re-layouts, shards(): jnp.concatenate([tap_terms, jnp.sum(grad_pre * normed, 0)[None], jnp.sum(...  3.82 us
  transfers between devices with their start and end apart: 5, of which 2 were waited for; matrix products, arithmetic and copies ran while one was open for 8% of the time, Pallas kernels for 0%

commit v1 on v0

v1 whole, which is shorter than its diff:
```python
import functools
import math

import jax
import jax.numpy as jnp
from jax import lax
from jax.experimental import pallas as pl
from jax.experimental.pallas import tpu as pltpu
from jax.sharding import PartitionSpec as P

EPS = 1e-05
LANES = 128
F32 = jnp.float32
BF16 = jnp.bfloat16
EXACT = lax.Precision.HIGHEST
VMEM = pl.BlockSpec(memory_space=pltpu.VMEM)
SMEM = pl.BlockSpec(memory_space=pltpu.SMEM)
HBM = pl.BlockSpec(memory_space=pltpu.HBM)


def up(value, step):
    return -(-value // step) * step


def call(body, name, outs, args, aliases=None, flops=0, specs=None, grid=None, limit=24):
    return pl.pallas_call(
        body,
        name=name,
        out_shape=[jax.ShapeDtypeStruct(shape, dtype) for shape, dtype in outs],
        in_specs=specs if specs else [VMEM] * len(args),
        out_specs=[VMEM] * len(outs),
        input_output_aliases=aliases or {},
        grid=grid or (),
        compiler_params=pltpu.CompilerParams(vmem_limit_bytes=limit * 2**20),
        cost_estimate=pl.CostEstimate(flops=flops, bytes_accessed=0, transcendentals=0),
    )(*args)


def gate_and_mix(
    pad,
    tile,
    flags,
    value_hbm,
    gate_hbm,
    grads_hbm,
    w_hbm,
    gated,
    mix,
    send_even,
    send_odd,
    value,
    gate,
    grads,
    w,
    sems,
):
    rows, channels = value.shape
    first = [
        pltpu.make_async_copy(source, target, sems.at[at])
        for at, (source, target) in enumerate(
            ((gate_hbm, gate), (value_hbm, value), (grads_hbm, grads))
        )
    ]
    weights = [
        pltpu.make_async_copy(
            w_hbm.at[pl.ds(at, tile), :], w.at[pl.ds(at, tile), :], sems.at[3 + at // tile]
        )
        for at in range(0, channels, tile)
    ]
    for copy in first + weights:
        copy.start()
    first[0].wait()
    first[1].wait()
    odd = flags[0] == 1
    for block in range(channels // LANES):
        lanes = slice(block * LANES, (block + 1) * LANES)
        sig = jax.nn.sigmoid(gate[:, lanes].astype(F32))
        product = (value[:, lanes].astype(F32) * sig).astype(BF16)
        gated[block, 2 * pad : 2 * pad + rows, :] = product.astype(F32)
        top = product[: 2 * pad]
        bottom = product[rows - 2 * pad :]
        send_even[: 2 * pad, lanes] = jnp.where(odd, top, bottom)
        send_odd[: 2 * pad, lanes] = jnp.where(odd, bottom, top)
    first[2].wait()
    for index, copy in enumerate(weights):
        copy.wait()
        mixed = lax.dot_general(
            grads[...],
            w[index * tile : (index + 1) * tile, :],
            (((1,), (1,)), ((), ())),
            preferred_element_type=F32,
        )
        for part in range(tile // LANES):
            lanes = slice(part * LANES, (part + 1) * LANES)
            mix[index * (tile // LANES) + part, pad : pad + rows, :] = mixed[:, lanes]
        top = mixed[:pad].astype(BF16)
        bottom = mixed[rows - pad :].astype(BF16)
        lanes = slice(index * tile, (index + 1) * tile)
        send_even[2 * pad :, lanes] = jnp.where(odd, top, bottom)
        send_odd[2 * pad :, lanes] = jnp.where(odd, bottom, top)


def conv_rows(taps, source, block, lanes, first, count, shift):
    total = jnp.zeros((count, LANES), F32)
    for tap in range(taps.shape[0]):
        total = total + taps[pl.ds(tap, 1), lanes] * source[block, pl.ds(first + tap + shift, count), :]
    return total


def pieces(first, last, most):
    count = -(-(last - first) // most)
    size = up(-(-(last - first) // count), 8)
    return [(at, min(size, last - at)) for at in range(first, last, size)]


def conv_inner(pad, gated, taps, out):
    blocks, height, _ = out.shape
    shift = pad - taps.shape[0] // 2

    def body(block, carry):
        lanes = pl.ds(pl.multiple_of(block * LANES, LANES), LANES)
        for at, count in pieces(2 * pad, height - 2 * pad, 56):
            out[block, at : at + count, :] = conv_rows(taps, gated, block, lanes, at, count, shift)
        return carry

    lax.fori_loop(0, blocks, body, 0)


def lane_sums(part):
    ones = jnp.ones((8, LANES), F32)
    return lax.dot_general(
        ones, part, (((1,), (1,)), ((), ())), precision=EXACT, preferred_element_type=F32
    )[0:1]


def spread(line):
    first = (lax.broadcasted_iota(jnp.int32, (8, LANES), 0) == 0).astype(F32)
    rows = jnp.concatenate([line, jnp.zeros((7, line.shape[1]), F32)], 0)
    return lax.dot_general(
        rows, first, (((0,), (0,)), ((), ())), precision=EXACT, preferred_element_type=F32
    )


def conv_edges(
    pad, flags, from_even, from_odd, taps, gated_in, mix_in, conv_in, gated, mix, conv, stats, part
):
    blocks, height, _ = conv.shape
    shift = pad - taps.shape[0] // 2
    odd = flags[0] == 1

    def fill(block, carry):
        lanes = pl.ds(pl.multiple_of(block * LANES, LANES), LANES)
        even_rows = from_even[:, lanes].astype(F32)
        odd_rows = from_odd[:, lanes].astype(F32)
        low = jnp.where(odd, even_rows, odd_rows)
        high = jnp.where(odd, odd_rows, even_rows)
        gated[block, : 2 * pad, :] = low[: 2 * pad]
        gated[block, height :, :] = high[: 2 * pad]
        mix[block, :pad, :] = low[2 * pad :]
        mix[block, height - pad :, :] = high[2 * pad :]
        for at in (0, height - 2 * pad):
            conv[block, at : at + 2 * pad, :] = conv_rows(
                taps, gated, block, lanes, at, 2 * pad, shift
            )
        return carry

    lax.fori_loop(0, blocks, fill, 0)

    def sums(chunk, carry):
        rows = pl.ds(pl.multiple_of(chunk * 16, 16), 16)
        first = jnp.zeros((16, LANES), F32)
        second = jnp.zeros((16, LANES), F32)
        for block in range(blocks):
            value = conv[block, rows, :]
            first = first + value
            second = second + value * value
        part[0, rows, :] = first
        part[1, rows, :] = second
        return carry

    lax.fori_loop(0, height // 16, sums, 0)
    stats[0:1, :] = lane_sums(part[0])
    stats[1:2, :] = lane_sums(part[1])


def moments(mine, other, width):
    mean = (mine[0:1, :] + other[0:1, :]) / width
    var = (mine[1:2, :] + other[1:2, :]) / width - mean * mean
    return mean, lax.rsqrt(var + EPS)


def norm_back(pad, width, conv, mix, stats, stats_other, gain, shift, normed, grad, second, sums, part, line):
    blocks, height, _ = conv.shape
    mean, inv = moments(stats, stats_other, width)
    line[0] = spread(mean)
    line[1] = spread(inv)

    def chunk_rows(rows, keep):
        mean_rows = line[0, rows, :]
        inv_rows = line[1, rows, :]
        first = jnp.zeros((16, LANES), F32)
        other = jnp.zeros((16, LANES), F32)
        kept = []
        for block in range(blocks):
            lanes = slice(block * LANES, (block + 1) * LANES)
            norm = (conv[block, rows, :] - mean_rows) * inv_rows
            gain_row = gain[:, lanes]
            pre = norm * gain_row + shift[:, lanes]
            sig = jax.nn.sigmoid(pre)
            grad_pre = mix[block, rows, :] * sig * (1.0 + pre * (1.0 - sig))
            grad_norm = grad_pre * gain_row
            normed[block, rows, :] = norm
            grad[block, rows, :] = grad_norm
            first = first + grad_norm
            other = other + grad_norm * norm
            if keep:
                product = grad_pre * norm
                kept += [product[:8] + product[8:], grad_pre[:8] + grad_pre[8:]]
        part[0, rows, :] = first
        part[1, rows, :] = other
        return kept

    for at in range(0, pad, 16):
        chunk_rows(pl.ds(at, 16), False)
        chunk_rows(pl.ds(height - pad + at, 16), False)

    def body(chunk, carry):
        kept = chunk_rows(pl.ds(pl.multiple_of(pad + chunk * 16, 16), 16), True)
        return tuple(old + new for old, new in zip(carry, kept))

    zero = tuple(jnp.zeros((8, LANES), F32) for _ in range(2 * blocks))
    totals = lax.fori_loop(0, (height - 2 * pad) // 16, body, zero)
    for block in range(blocks):
        for which in range(2):
            sums[which, block : block + 1, :] = jnp.sum(totals[2 * block + which], 0, keepdims=True)
    second[0:1, :] = lane_sums(part[0])
    second[1:2, :] = lane_sums(part[1])


def tap_sums(
    pad, width, kernel, flags, normed, grad, stats, stats_other, second, second_other, sums, gated, grad_conv, packed, line, raw
):
    blocks, height, _ = normed.shape
    rows = height - 2 * pad
    each = up(kernel + 1, 16)
    shift = pad - kernel // 2
    _, inv = moments(stats, stats_other, width)
    line[0] = spread(inv)
    line[1] = spread((second[0:1, :] + second_other[0:1, :]) / width)
    line[2] = spread((second[1:2, :] + second_other[1:2, :]) / width)
    raw[...] = jnp.zeros_like(raw)

    def finish(block, carry):
        for at, count in pieces(0, height, 48):
            span = slice(at, at + count)
            grad_conv[block, span, :] = line[0, span, :] * (
                grad[block, span, :] - line[1, span, :] - normed[block, span, :] * line[2, span, :]
            )
        return carry

    lax.fori_loop(0, blocks, finish, 0)

    @pl.when(flags[1] == 1)
    def _():
        grad_conv[:, :pad, :] = jnp.zeros((blocks, pad, LANES), F32)

    @pl.when(flags[2] == 1)
    def _():
        grad_conv[:, height - pad :, :] = jnp.zeros((blocks, pad, LANES), F32)

    def body(block, carry):
        base = pl.multiple_of(block * each, each)
        for low in range(0, kernel, 8):
            taps = range(low, min(low + 8, kernel))
            totals = [jnp.zeros((8, LANES), F32) for _ in taps]
            for at in range(0, rows, 32):
                own = grad_conv[block, pad + at : pad + at + 32, :]
                for index, tap in enumerate(taps):
                    term = own * gated[block, pl.ds(pad + at + tap + shift, 32), :]
                    totals[index] = totals[index] + (
                        (term[0:8] + term[8:16]) + (term[16:24] + term[24:32])
                    )
            for index, tap in enumerate(taps):
                raw[pl.ds(base + tap, 1), :] = jnp.sum(totals[index], 0, keepdims=True)
        raw[pl.ds(base + kernel, 1), :] = sums[0, pl.ds(block, 1), :]
        return carry

    lax.fori_loop(0, blocks, body, 0)
    raw[blocks * each : blocks * each + blocks, :] = sums[1]
    packed[...] = raw[...].astype(BF16)


def conv_back(pad, grad_conv, taps, value, gate, d_value, d_gate):
    blocks, height, _ = grad_conv.shape
    rows = height - 2 * pad
    kernel = taps.shape[0]
    top = pad + kernel // 2

    def body(block, carry):
        lanes = pl.ds(pl.multiple_of(block * LANES, LANES), LANES)
        for at, count in pieces(0, rows, 64):
            total = jnp.zeros((count, LANES), F32)
            for tap in range(kernel):
                total = total + taps[pl.ds(tap, 1), lanes] * grad_conv[
                    block, pl.ds(at + top - tap, count), :
                ]
            sig = jax.nn.sigmoid(gate[at : at + count, lanes].astype(F32))
            scaled = total * sig
            d_value[at : at + count, lanes] = scaled.astype(BF16)
            d_gate[at : at + count, lanes] = (
                scaled * value[at : at + count, lanes].astype(F32) * (1.0 - sig)
            ).astype(BF16)
        return carry

    lax.fori_loop(0, blocks, body, 0)


def unpack(scale, kernel, mine, other, d_taps, d_gain, d_shift):
    each = up(kernel + 1, 16)
    blocks = d_gain.shape[0]
    total = (mine[...].astype(F32) + other[...].astype(F32)) * scale
    for block in range(blocks):
        base = block * each
        d_taps[:, block * LANES : (block + 1) * LANES] = total[base : base + kernel]
        d_gain[block : block + 1, :] = total[base + kernel : base + kernel + 1]
    d_shift[...] = total[blocks * each : blocks * each + blocks]


def swap_cores(line):
    count = lax.axis_size("tp")
    if count == 1:
        return jnp.zeros_like(line)
    assert count == 2
    return lax.ppermute(line, "tp", [(0, 1), (1, 0)])


def radices(count):
    found = []
    step = 1
    odd = 3
    while (count // step) % 2 == 0:
        step *= 2
    twos = step
    while step < count:
        while (count // step) % odd == 0:
            found.append((odd, step // twos))
            step *= odd
        odd += 2
    step = count // twos
    while step < count:
        found.append((2, step))
        step *= 2
    return found


def turn(count, radix, step, shift_by):
    pairs = []
    for i in range(count):
        digit = (i // step) % radix
        pairs.append((i, i + ((digit + shift_by) % radix - digit) * step))
    return pairs


def shards(value_in, gate_in, taps, gain, shift, w_out, grad_out):
    kernel, channels = taps.shape
    rows = value_in.shape[0]
    depth = grad_out.shape[1]
    count = lax.axis_size("sp")
    width = channels * lax.axis_size("tp")
    blocks = channels // LANES
    pad = up(kernel // 2 + 1, 16)
    height = rows + 2 * pad
    index = lax.axis_index("sp")
    flags = jnp.stack(
        [index % 2, (index == 0).astype(jnp.int32), (index == count - 1).astype(jnp.int32)]
    ).astype(jnp.int32)
    tile = 2 * LANES if channels % (2 * LANES) == 0 else LANES
    each = up(kernel + 1, 16)

    gated, mix, send_even, send_odd = pl.pallas_call(
        functools.partial(gate_and_mix, pad, tile),
        name="gate_and_mix",
        out_shape=[
            jax.ShapeDtypeStruct((blocks, height + 2 * pad, LANES), F32),
            jax.ShapeDtypeStruct((blocks, height, LANES), F32),
            jax.ShapeDtypeStruct((3 * pad, channels), BF16),
            jax.ShapeDtypeStruct((3 * pad, channels), BF16),
        ],
        in_specs=[SMEM] + [HBM] * 4,
        out_specs=[VMEM] * 4,
        scratch_shapes=[
            pltpu.VMEM((rows, channels), BF16),
            pltpu.VMEM((rows, channels), BF16),
            pltpu.VMEM((rows, depth), BF16),
            pltpu.VMEM((channels, depth), BF16),
            pltpu.SemaphoreType.DMA((3 + channels // tile,)),
        ],
        compiler_params=pltpu.CompilerParams(vmem_limit_bytes=24 * 2**20),
    )(flags, *(pltpu.with_memory_space_constraint(x, pltpu.HBM) for x in (value_in, gate_in, grad_out, w_out)))
    swap_odd = [(i, i + 1) for i in range(1, count - 1, 2)]
    swap_even = [(i, i + 1) for i in range(0, count - 1, 2)]
    from_odd = lax.ppermute(send_odd, "sp", swap_odd + [(b, a) for a, b in swap_odd])
    from_even = lax.ppermute(send_even, "sp", swap_even + [(b, a) for a, b in swap_even])
    conv_flops = 2 * kernel * rows * channels
    (inner,) = call(
        functools.partial(conv_inner, pad),
        "conv_inner",
        [((blocks, height, LANES), F32)],
        (gated, taps),
        flops=conv_flops,
    )
    gated, mix, conv, stats = pl.pallas_call(
        functools.partial(conv_edges, pad),
        name="conv_edges",
        out_shape=[
            jax.ShapeDtypeStruct(gated.shape, F32),
            jax.ShapeDtypeStruct(mix.shape, F32),
            jax.ShapeDtypeStruct(inner.shape, F32),
            jax.ShapeDtypeStruct((2, height), F32),
        ],
        in_specs=[SMEM] + [VMEM] * 6,
        out_specs=[VMEM] * 4,
        input_output_aliases={4: 0, 5: 1, 6: 2},
        scratch_shapes=[pltpu.VMEM((2, height, LANES), F32)],
        compiler_params=pltpu.CompilerParams(vmem_limit_bytes=24 * 2**20),
    )(flags, from_even, from_odd, taps, gated, mix, inner)
    stats_other = swap_cores(stats)
    normed, grad, second, sums = pl.pallas_call(
        functools.partial(norm_back, pad, width),
        name="norm_back",
        out_shape=[
            jax.ShapeDtypeStruct(conv.shape, F32),
            jax.ShapeDtypeStruct(conv.shape, F32),
            jax.ShapeDtypeStruct((2, height), F32),
            jax.ShapeDtypeStruct((2, blocks, LANES), F32),
        ],
        in_specs=[VMEM] * 6,
        out_specs=[VMEM] * 4,
        scratch_shapes=[pltpu.VMEM((2, height, LANES), F32), pltpu.VMEM((2, height, LANES), F32)],
        compiler_params=pltpu.CompilerParams(vmem_limit_bytes=24 * 2**20),
    )(conv, mix, stats, stats_other, gain[None], shift[None])
    second_other = swap_cores(second)
    packed_rows = up(blocks * each + blocks, 16)
    grad_conv, packed = pl.pallas_call(
        functools.partial(tap_sums, pad, width, kernel),
        name="tap_sums",
        out_shape=[
            jax.ShapeDtypeStruct(conv.shape, F32),
            jax.ShapeDtypeStruct((packed_rows, LANES), BF16),
        ],
        in_specs=[SMEM] + [VMEM] * 8,
        out_specs=[VMEM] * 2,
        scratch_shapes=[pltpu.VMEM((3, height, LANES), F32), pltpu.VMEM((packed_rows, LANES), F32)],
        compiler_params=pltpu.CompilerParams(vmem_limit_bytes=24 * 2**20),
    )(flags, normed, grad, stats, stats_other, second, second_other, sums, gated)
    d_value, d_gate = call(
        functools.partial(conv_back, pad),
        "conv_back",
        [((rows, channels), BF16), ((rows, channels), BF16)],
        (grad_conv, taps, value_in, gate_in),
        flops=conv_flops,
    )
    mine = packed
    other = None
    for at, (radix, step) in enumerate(radices(count)):
        digit = (index // step) % radix
        arrived = [
            lax.ppermute(mine, "sp", turn(count, radix, step, shift_by))
            for shift_by in range(1, radix)
        ]
        if radix == 2:
            if step * radix == count:
                other = arrived[0]
                break
            total = mine.astype(F32) + arrived[0].astype(F32)
        else:
            total = jnp.zeros(mine.shape, F32)
            held = [mine] + arrived
            for place in range(radix):
                term = held[0]
                for away in range(1, radix):
                    term = jnp.where((digit - away) % radix == place, held[away], term)
                total = total + term.astype(F32)
        mine = lax.reduce_precision(total, 8, 7).astype(BF16)
    if other is None:
        other = jnp.zeros_like(mine)
    d_taps, d_gain, d_shift = call(
        functools.partial(unpack, 1.0 / math.sqrt(rows * count), kernel),
        "unpack",
        [((kernel, channels), F32), ((blocks, LANES), F32), ((blocks, LANES), F32)],
        (mine, other),
    )
    return (d_value, d_gate, d_taps, d_gain.reshape(channels), d_shift.reshape(channels))


def solution(mesh):
    return jax.shard_map(
        shards,
        mesh=mesh,
        in_specs=(
            P("sp", "tp"),
            P("sp", "tp"),
            P(None, "tp"),
            P("tp"),
            P("tp"),
            P("tp", None),
            P("sp", None),
        ),
        out_specs=(P("sp", "tp"), P("sp", "tp"), P(None, "tp"), P("tp"), P("tp")),
        check_vma=False,
    )
```

time: 176 us -> 49.3 us (0.28)
  waiting for transfers between devices: 106 us -> 9.44 us
  other arithmetic: 24.5 us -> 0.14 us
  Pallas kernels: 0 us -> 20 us
  between operations: 14.5 us -> 0.7 us
  local copies, waits for them, and re-layouts: 7.63 us -> 0.02 us
  starting transfers between devices: 12.4 us -> 18.8 us
  matrix products: 5.53 us -> 0 us
  blocking collectives: 4.91 us -> 0 us
    psum x1 -> x0, waiting for transfers between devices: 101 us -> none  [shards(): summed = lax.psum(stacked, 'sp')]
    pallas_call x0 -> x7, Pallas kernels: none -> 20 us  [the longest x3 6.9 us: call(): pl.pallas_call(body, name=name, out_shape=[jax.ShapeDtypeStruct(shape, dt...]
    reduce_sum x3 -> x0, other arithmetic: 12.9 us -> none  [the longest x2 7.23 us: shards(): jnp.sum(own_grad * gated_float[offset:offset + rows], 0)]
    convert_element_type x4 -> x3, other arithmetic: 10.9 us -> 0.07 us  [shards(): mine = lax.reduce_precision(total, 8, 7).astype(BF16)]
    ppermute x4 -> x8, starting transfers between devices: 12.4 us -> 18.8 us  [the longest x4 14.9 us: shards(): lax.ppermute(mine, 'sp', turn(count, radix, step, shift_by))]
    dot_general x1 -> x0, matrix products: 5.53 us -> none  [norm_backward(): lax.dot_general(grad_rows, w_out, (((1,), (1,)), ((), ())), preferred_ele...]
    ppermute x4 -> x8, waiting for transfers between devices: 4.19 us -> 9.44 us  [the longest x4 7.09 us: shards(): lax.ppermute(mine, 'sp', turn(count, radix, step, shift_by))]
    psum x2 -> x0, blocking collectives: 4.91 us -> none  [the longest x1 2.47 us: norm_backward(): lax.psum((jnp.sum(conv_out, 1), jnp.sum(conv_out * conv_out, 1)), 'tp')]
  transfers between devices with their start and end apart: 5 -> 8, of which waited for: 2 -> 6; matrix products, arithmetic and copies ran while one was open for 8% -> 0% of each run, Pallas kernels for 0% -> 13%
where the time goes in v1:
time: 49.3 us; the launch traced here: 49.1 us
  Pallas kernels  20 us (41%)
  starting transfers between devices  18.8 us (38%)
  waiting for transfers between devices  9.44 us (19%)
  between operations  0.7 us (1%)
    ppermute x4, starting transfers between devices, shards(): lax.ppermute(mine, 'sp', turn(count, radix, step, shift_by))  14.9 us
    ppermute x4, waiting for transfers between devices, shards(): lax.ppermute(mine, 'sp', turn(count, radix, step, shift_by))  7.09 us
    pallas_call x3, Pallas kernels, call(): pl.pallas_call(body, name=name, out_shape=[jax.ShapeDtypeStruct(shape, dt...  6.9 us
    pallas_call x1, Pallas kernels, shards(): pl.pallas_call(functools.partial(gate_and_mix, pad, tile), name='gate_and...  5.37 us
    pallas_call x1, Pallas kernels, shards(): pl.pallas_call(functools.partial(tap_sums, pad, width, kernel), name='tap...  4.21 us
    ppermute x1, starting transfers between devices, shards(): lax.ppermute(send_even, 'sp', swap_even + [(b, a) for a, b in swap_even])  3.03 us
    ppermute x2, waiting for transfers between devices, swap_cores(): return lax.ppermute(line, 'tp', [(0, 1), (1, 0)])  2.18 us
    pallas_call x1, Pallas kernels, shards(): pl.pallas_call(functools.partial(conv_edges, pad), name='conv_edges', out...  1.81 us
  transfers between devices with their start and end apart: 8, of which 6 were waited for; matrix products, arithmetic and copies ran while one was open for 0% of the time, Pallas kernels for 13%

profile of v1, /device:TPU:0, one launch (start us, length us, event | category | flops | bytes accessed | tf_op | source)
XLA Modules:
  0.0 49.1 jit_solution(18329950880162703182)
XLA Ops:
  0.6 0.1 pad_add_fusion.flags
  0.7 0.0 copy-start.2
  0.7 5.4 %gate_and_mix.1 = (f32[8,320,128]{2,1,0:T(8,128)S(1)}, f32[8,288,128]{2,1,0:T(8,128)S(1)}, bf16[48,1024]{1,0:T(8,128)(2,1)S(1)}, bf16[48,1024]{1,0:T(8,128)(2,1)S(1)}) custom-call(s32[3]{0:T(128)S(1)} %pad_add_fusion.flags, bf16[256,1024]{1,0:T(8,128)(2,1)} %value.1, bf16[256,1024]{1,0:T(8,128)(2,1)} %gate.1, bf16[256,2048]{1,0:T(8,128)(2,1)} %grads_hbm.1, ...), custom_call_target="tpu_custom_call" | custom-call | tf_op jit(solution)/shard_map/gate_and_mix/pallas_call | solution.py:380
  6.1 3.0 %collective-permute-start = (bf16[48,1024]{1,0:T(8,128)(2,1)S(1)}, bf16[48,1024]{1,0:T(8,128)(2,1)S(1)}, u32[]{:S(2)}, u32[]{:S(2)}) collective-permute-start(bf16[48,1024]{1,0:T(8,128)(2,1)S(1)} %get-tuple-element.24), channel_id=1, source_target_pairs={{0,2},{4,6},{8,10},{12,14},{16,18},{20,22},{24,26},{28,30},{2,0},{... | collective-permute-start | bytes 294920 | tf_op jit(solution)/shard_map/ppermute | solution.py:403
  9.1 0.7 %collective-permute-start.1 = (bf16[48,1024]{1,0:T(8,128)(2,1)S(1)}, bf16[48,1024]{1,0:T(8,128)(2,1)S(1)}, u32[]{:S(2)}, u32[]{:S(2)}) collective-permute-start(bf16[48,1024]{1,0:T(8,128)(2,1)S(1)} %get-tuple-element.25), channel_id=1, source_target_pairs={{2,4},{6,8},{10,12},{14,16},{18,20},{22,24},{26,28},{4,2},{8,6},{1... | collective-permute-start | bytes 294920 | tf_op jit(solution)/shard_map/ppermute | solution.py:402
  9.8 0.0 copy-done.2
  9.8 2.0 %conv_inner.1.conv_in = f32[8,288,128]{2,1,0:T(8,128)S(1)} custom-call(f32[8,320,128]{2,1,0:T(8,128)S(1)} %get-tuple-element.26.gated.gated_in, f32[31,1024]{1,0:T(8,128)S(1)} %copy-done.2), custom_call_target="tpu_custom_call" | custom-call | flops 16252928 | tf_op jit(solution)/shard_map/conv_inner/pallas_call | solution.py:26
  11.8 0.2 collective-permute-done.from_even
  11.9 0.0 collective-permute-done.1.from_odd
  11.9 0.0 copy-start.3
  11.9 0.0 copy-start.4
  11.9 1.8 %conv_edges.1 = (f32[8,320,128]{2,1,0:T(8,128)S(1)}, f32[8,288,128]{2,1,0:T(8,128)S(1)}, f32[8,288,128]{2,1,0:T(8,128)S(1)}, f32[2,288]{1,0:T(2,128)S(1)}) custom-call(s32[3]{0:T(128)S(1)} %pad_add_fusion.flags, bf16[48,1024]{1,0:T(8,128)(2,1)S(1)} %collective-permute-done.from_even, ...), custom_call_target="tpu_custom_call", output_to_operand_aliasing={{0}: (4, {}), {1}: (5, {}), {2}: (6, {})} | custom-call | tf_op jit(solution)/shard_map/conv_edges/pallas_call | solution.py:412
  13.7 0.0 collective-permute-start.2
  13.7 1.2 %collective-permute-done.2.stats_other = f32[2,288]{1,0:T(2,128)S(1)} collective-permute-done((f32[2,288]{1,0:T(2,128)S(1)}, f32[2,288]{1,0:T(2,128)S(1)}, u32[]{:S(2)}, u32[]{:S(2)}) %collective-permute-start.2) | collective-permute-done | bytes 2336 | tf_op jit(solution)/shard_map/ppermute | solution.py:334
  14.9 0.0 copy-done.3
  14.9 0.0 copy-done.4
  14.9 1.7 %norm_back.1 = (f32[8,288,128]{2,1,0:T(8,128)S(1)}, f32[8,288,128]{2,1,0:T(8,128)S(1)}, f32[2,288]{1,0:T(2,128)S(1)}, f32[2,8,128]{2,1,0:T(8,128)S(1)}) custom-call(f32[8,288,128]{2,1,0:T(8,128)S(1)} %get-tuple-element.28.conv, f32[8,288,128]{2,1,0:T(8,128)S(1)} %get-tuple-element.29.mix, f32[2,288]{1,0:T(2,128)S(1)} %get-tuple-element.30.stats, ...), custom_call_target="tpu_custom_call" | custom-call | tf_op jit(solution)/shard_map/norm_back/pallas_call | solution.py:428
  16.7 0.2 collective-permute-start.3
  16.9 1.0 %collective-permute-done.3.second_other = f32[2,288]{1,0:T(2,128)S(1)} collective-permute-done((f32[2,288]{1,0:T(2,128)S(1)}, f32[2,288]{1,0:T(2,128)S(1)}, u32[]{:S(2)}, u32[]{:S(2)}) %collective-permute-start.3) | collective-permute-done | bytes 2336 | tf_op jit(solution)/shard_map/ppermute | solution.py:334
  17.9 4.2 %tap_sums.1 = (f32[8,288,128]{2,1,0:T(8,128)S(1)}, bf16[272,128]{1,0:T(8,128)(2,1)S(1)}) custom-call(s32[3]{0:T(128)S(1)} %pad_add_fusion.flags, f32[8,288,128]{2,1,0:T(8,128)S(1)} %get-tuple-element.31.normed, f32[8,288,128]{2,1,0:T(8,128)S(1)} %get-tuple-element.32.grad, f32[2,288]{1,0:T(2,128)S(1)} %get-tuple-element.30.stats, ...), custom_call_target="tpu_custom_call" | custom-call | tf_op jit(solution)/shard_map/tap_sums/pallas_call | solution.py:444
  22.1 4.9 %collective-permute-start.4 = (bf16[272,128]{1,0:T(8,128)(2,1)S(1)}, bf16[272,128]{1,0:T(8,128)(2,1)S(1)}, u32[]{:S(2)}, u32[]{:S(2)}) collective-permute-start(bf16[272,128]{1,0:T(8,128)(2,1)S(1)} %get-tuple-element.39), channel_id=1, source_target_pairs={{0,2},{2,0},{4,6},{6,4},{8,10},{10,8},{12,14},{14,12},{16,18},{18,... | collective-permute-start | bytes 208904 | tf_op jit(solution)/shard_map/ppermute | solution.py:468
  27.0 2.5 %collective-permute-done.4 = bf16[272,128]{1,0:T(8,128)(2,1)S(1)} collective-permute-done((bf16[272,128]{1,0:T(8,128)(2,1)S(1)}, bf16[272,128]{1,0:T(8,128)(2,1)S(1)}, u32[]{:S(2)}, u32[]{:S(2)}) %collective-permute-start.4) | collective-permute-done | bytes 69664 | tf_op jit(solution)/shard_map/ppermute | solution.py:468
  29.6 3.1 %collective-permute-start.5 = (bf16[272,128]{1,0:T(8,128)(2,1)S(1)}, bf16[272,128]{1,0:T(8,128)(2,1)S(1)}, u32[]{:S(2)}, u32[]{:S(2)}) collective-permute-start(bf16[272,128]{1,0:T(8,128)(2,1)S(1)} %reduce-precision_convert_fusion.2), channel_id=1, source_target_pairs={{0,4},{2,6},{4,0},{6,2},{8,12},{10,14},{12,8},{14,10},{16,20},{18,... | collective-permute-start | bytes 208904 | tf_op jit(solution)/shard_map/ppermute | solution.py:468
  32.7 2.3 %collective-permute-done.5 = bf16[272,128]{1,0:T(8,128)(2,1)S(1)} collective-permute-done((bf16[272,128]{1,0:T(8,128)(2,1)S(1)}, bf16[272,128]{1,0:T(8,128)(2,1)S(1)}, u32[]{:S(2)}, u32[]{:S(2)}) %collective-permute-start.5) | collective-permute-done | bytes 69664 | tf_op jit(solution)/shard_map/ppermute | solution.py:468
  35.0 3.0 %collective-permute-start.6 = (bf16[272,128]{1,0:T(8,128)(2,1)S(1)}, bf16[272,128]{1,0:T(8,128)(2,1)S(1)}, u32[]{:S(2)}, u32[]{:S(2)}) collective-permute-start(bf16[272,128]{1,0:T(8,128)(2,1)S(1)} %reduce-precision_convert_fusion.1), channel_id=1, source_target_pairs={{0,8},{2,10},{4,12},{6,14},{8,0},{10,2},{12,4},{14,6},{16,24},{18,... | collective-permute-start | bytes 208904 | tf_op jit(solution)/shard_map/ppermute | solution.py:468
  38.0 2.3 %collective-permute-done.6 = bf16[272,128]{1,0:T(8,128)(2,1)S(1)} collective-permute-done((bf16[272,128]{1,0:T(8,128)(2,1)S(1)}, bf16[272,128]{1,0:T(8,128)(2,1)S(1)}, u32[]{:S(2)}, u32[]{:S(2)}) %collective-permute-start.6) | collective-permute-done | bytes 69664 | tf_op jit(solution)/shard_map/ppermute | solution.py:468
  40.3 3.8 %collective-permute-start.7 = (bf16[272,128]{1,0:T(8,128)(2,1)S(1)}, bf16[272,128]{1,0:T(8,128)(2,1)S(1)}, u32[]{:S(2)}, u32[]{:S(2)}) collective-permute-start(bf16[272,128]{1,0:T(8,128)(2,1)S(1)} %reduce-precision_convert_fusion.mine), channel_id=1, source_target_pairs={{0,16},{2,18},{4,20},{6,22},{8,24},{10,26},{12,28},{14,30},{16,0},... | collective-permute-start | bytes 208904 | tf_op jit(solution)/shard_map/ppermute | solution.py:468
  44.1 0.0 copy-done
  44.1 0.0 copy-done.1
  44.2 4.3 %conv_back.1 = (bf16[256,1024]{1,0:T(8,128)(2,1)}, bf16[256,1024]{1,0:T(8,128)(2,1)}) custom-call(f32[8,288,128]{2,1,0:T(8,128)S(1)} %get-tuple-element.36.grad_conv, f32[31,1024]{1,0:T(8,128)S(1)} %copy-done.2, bf16[256,1024]{1,0:T(8,128)(2,1)S(1)} %copy-done, bf16[256,1024]{1,0:T(8,128)(2,1)S(1)} %copy-done.1), custom_call_target="tpu_custom_call" | custom-call | flops 16252928 | tf_op jit(solution)/shard_map/conv_back/pallas_call | solution.py:26
  48.4 0.0 collective-permute-done.7.other
  48.4 0.7 %unpack.1 = (f32[31,1024]{1,0:T(8,128)}, f32[8,128]{1,0:T(8,128)}, f32[8,128]{1,0:T(8,128)}) custom-call(bf16[272,128]{1,0:T(8,128)(2,1)S(1)} %reduce-precision_convert_fusion.mine, bf16[272,128]{1,0:T(8,128)(2,1)S(1)} %collective-permute-done.7.other), custom_call_target="tpu_custom_call" | custom-call | tf_op jit(solution)/shard_map/unpack/pallas_call | solution.py:26
  (5 shorter events, 0.1 us)
Async XLA Ops:
  0.7 9.1 %copy-start.2 = (f32[31,1024]{1,0:T(8,128)S(1)}, f32[31,1024]{1,0:T(8,128)}, u32[]{:S(2)}) copy-start(f32[31,1024]{1,0:T(8,128)} %taps.5) | copy-start | bytes 380932
  6.1 5.8 %collective-permute-start = (bf16[48,1024]{1,0:T(8,128)(2,1)S(1)}, bf16[48,1024]{1,0:T(8,128)(2,1)S(1)}, u32[]{:S(2)}, u32[]{:S(2)}) collective-permute-start(bf16[48,1024]{1,0:T(8,128)(2,1)S(1)} %get-tuple-element.24), channel_id=1, source_target_pairs={{0,2},{4,6},{8,10},{12,14},{16,18},{20,22},{24,26},{28,30},{2,0},{... | collective-permute-start | bytes 294920 | tf_op jit(solution)/shard_map/ppermute | solution.py:403
  9.1 2.8 %collective-permute-start.1 = (bf16[48,1024]{1,0:T(8,128)(2,1)S(1)}, bf16[48,1024]{1,0:T(8,128)(2,1)S(1)}, u32[]{:S(2)}, u32[]{:S(2)}) collective-permute-start(bf16[48,1024]{1,0:T(8,128)(2,1)S(1)} %get-tuple-element.25), channel_id=1, source_target_pairs={{2,4},{6,8},{10,12},{14,16},{18,20},{22,24},{26,28},{4,2},{8,6},{1... | collective-permute-start | bytes 294920 | tf_op jit(solution)/shard_map/ppermute | solution.py:402
  11.9 3.0 %copy-start.3 = (f32[1024]{0:T(1024)S(1)}, f32[1024]{0:T(1024)}, u32[]{:S(2)}) copy-start(f32[1024]{0:T(1024)} %param.10) | copy-start | bytes 12292
  11.9 3.0 %copy-start.4 = (f32[1024]{0:T(1024)S(1)}, f32[1024]{0:T(1024)}, u32[]{:S(2)}) copy-start(f32[1024]{0:T(1024)} %param.11) | copy-start | bytes 12292
  13.7 1.2 %collective-permute-start.2 = (f32[2,288]{1,0:T(2,128)S(1)}, f32[2,288]{1,0:T(2,128)S(1)}, u32[]{:S(2)}, u32[]{:S(2)}) collective-permute-start(f32[2,288]{1,0:T(2,128)S(1)} %get-tuple-element.30.stats), channel_id=1, source_target_pairs={{0,1},{1,0},{2,3},{3,2},{4,5},{5,4},{6,7},{7,6},{8,9},{9,8},{10,11... | collective-permute-start | bytes 6920 | tf_op jit(solution)/shard_map/ppermute | solution.py:334
  16.7 1.2 %collective-permute-start.3 = (f32[2,288]{1,0:T(2,128)S(1)}, f32[2,288]{1,0:T(2,128)S(1)}, u32[]{:S(2)}, u32[]{:S(2)}) collective-permute-start(f32[2,288]{1,0:T(2,128)S(1)} %get-tuple-element.33.second), channel_id=1, source_target_pairs={{0,1},{1,0},{2,3},{3,2},{4,5},{5,4},{6,7},{7,6},{8,9},{9,8},{10,11... | collective-permute-start | bytes 6920 | tf_op jit(solution)/shard_map/ppermute | solution.py:334
  17.9 26.3 %copy-start = (bf16[256,1024]{1,0:T(8,128)(2,1)S(1)}, bf16[256,1024]{1,0:T(8,128)(2,1)}, u32[]{:S(2)}) copy-start(bf16[256,1024]{1,0:T(8,128)(2,1)} %value.1) | copy-start | bytes 1572868
  17.9 26.3 %copy-start.1 = (bf16[256,1024]{1,0:T(8,128)(2,1)S(1)}, bf16[256,1024]{1,0:T(8,128)(2,1)}, u32[]{:S(2)}) copy-start(bf16[256,1024]{1,0:T(8,128)(2,1)} %gate.1) | copy-start | bytes 1572868
  22.1 7.5 %collective-permute-start.4 = (bf16[272,128]{1,0:T(8,128)(2,1)S(1)}, bf16[272,128]{1,0:T(8,128)(2,1)S(1)}, u32[]{:S(2)}, u32[]{:S(2)}) collective-permute-start(bf16[272,128]{1,0:T(8,128)(2,1)S(1)} %get-tuple-element.39), channel_id=1, source_target_pairs={{0,2},{2,0},{4,6},{6,4},{8,10},{10,8},{12,14},{14,12},{16,18},{18,... | collective-permute-start | bytes 208904 | tf_op jit(solution)/shard_map/ppermute | solution.py:468
  29.6 5.4 %collective-permute-start.5 = (bf16[272,128]{1,0:T(8,128)(2,1)S(1)}, bf16[272,128]{1,0:T(8,128)(2,1)S(1)}, u32[]{:S(2)}, u32[]{:S(2)}) collective-permute-start(bf16[272,128]{1,0:T(8,128)(2,1)S(1)} %reduce-precision_convert_fusion.2), channel_id=1, source_target_pairs={{0,4},{2,6},{4,0},{6,2},{8,12},{10,14},{12,8},{14,10},{16,20},{18,... | collective-permute-start | bytes 208904 | tf_op jit(solution)/shard_map/ppermute | solution.py:468
  35.0 5.3 %collective-permute-start.6 = (bf16[272,128]{1,0:T(8,128)(2,1)S(1)}, bf16[272,128]{1,0:T(8,128)(2,1)S(1)}, u32[]{:S(2)}, u32[]{:S(2)}) collective-permute-start(bf16[272,128]{1,0:T(8,128)(2,1)S(1)} %reduce-precision_convert_fusion.1), channel_id=1, source_target_pairs={{0,8},{2,10},{4,12},{6,14},{8,0},{10,2},{12,4},{14,6},{16,24},{18,... | collective-permute-start | bytes 208904 | tf_op jit(solution)/shard_map/ppermute | solution.py:468
  40.3 8.1 %collective-permute-start.7 = (bf16[272,128]{1,0:T(8,128)(2,1)S(1)}, bf16[272,128]{1,0:T(8,128)(2,1)S(1)}, u32[]{:S(2)}, u32[]{:S(2)}) collective-permute-start(bf16[272,128]{1,0:T(8,128)(2,1)S(1)} %reduce-precision_convert_fusion.mine), channel_id=1, source_target_pairs={{0,16},{2,18},{4,20},{6,22},{8,24},{10,26},{12,28},{14,30},{16,0},... | collective-permute-start | bytes 208904 | tf_op jit(solution)/shard_map/ppermute | solution.py:468
